TPU v7x, 32 devices: a whole 2x2x4 slice. The times are simulated.
32 devices in a mesh: ep: 8 (over z, x), tp: 4 (over y, core).
Axes of the slice: x: 2, y: 2, z: 4, core: 2. Of those that a mesh axis runs over, the one named last changes fastest.
Arguments:
- tokens: bfloat16 [32, 2048], P('ep'), may hold values from -6 to 6
- norm_gain: bfloat16 [2048], replicated, may hold values from 0.099609375 to 1.8984375
- in_weight: bfloat16 [2048, 1024], P(None, 'tp'), may hold values from -0.125 to 0.125
- decay_rate: float32 [64, 64], P('tp'), may hold values from 0.05 to 1
- frequency: float32 [64, 64], P('tp'), may hold values from -3 to 3
- log_step: float32 [64], P('tp'), may hold values from -2.3 to 0.7
- input_real: float32 [64, 64, 16], P('tp'), may hold values from -1.75 to 1.75
- input_imag: float32 [64, 64, 16], P('tp'), may hold values from -1.75 to 1.75
- output_real: float32 [64, 16, 64], P('tp'), may hold values from -0.5 to 0.5
- output_imag: float32 [64, 16, 64], P('tp'), may hold values from -0.5 to 0.5
- skip_gain: float32 [1024], P('tp'), may hold values from -3 to 3
- state_real: float32 [32, 64, 64], P('ep', 'tp'), may hold values from -6 to 6
- state_imag: float32 [32, 64, 64], P('ep', 'tp'), may hold values from -6 to 6
- out_weight: bfloat16 [1024, 2048], P('tp'), may hold values from -0.1875 to 0.1875
- ffn_gain: bfloat16 [2048], replicated, may hold values from 0.099609375 to 1.8984375
- expert_ids: int32 [32, 2], replicated, may hold values from 0 to 7, all different within a row; in each aligned block of 4 rows (0 to 3, 4 to 7, ...) at most 2 rows name the same one
- route_weights: float32 [32, 2], P('ep'), may hold values from 0.2 to 1
- gate_weight: bfloat16 [2048, 65536], P(None, ('ep', 'tp')), may hold values from -0.125 to 0.125
- up_weight: bfloat16 [2048, 65536], P(None, ('ep', 'tp')), may hold values from -0.125 to 0.125
- down_weight: bfloat16 [65536, 2048], P('ep', 'tp'), may hold values from -0.0625 to 0.0625
Outputs:
- mixed: bfloat16 [32, 2048], P('ep', 'tp')
- new_real: float32 [32, 64, 64], P('ep', 'tp')
- new_imag: float32 [32, 64, 64], P('ep', 'tp')
Inputs may be any that keep to these rules, and one draw needn't show every extreme that they name: `expert_ids`: the 2 experts of a row differ. In each aligned block of 4 rows (the rows of one index of ep) no expert is named by more than 2 rows, and in some blocks one expert is named by exactly 2 rows.
All inputs are finite; a program needn't handle non-finite values.
Results may differ from a plain program's by a relative error of at most 0.007.
Values may be sent and summed in bfloat16 or wider, within the bound.
A program may use at most 64 MiB of HBM per device.

v0:
```python
import jax
import jax.numpy as jnp
from jax import lax
from jax.sharding import PartitionSpec as P

EXPERTS = 8


EPSILON = 1e-06


def rms_scale(values, gain):
    floats = values.astype(jnp.float32)
    return (
        floats
        * lax.rsqrt(jnp.mean(floats * floats, axis=-1, keepdims=True) + EPSILON)
        * gain.astype(jnp.float32)
    )


def discretize(decay_rate, frequency, log_step, input_real, input_imag):
    step_size = jnp.exp(log_step)[:, None]
    lam_real = -decay_rate
    magnitude = jnp.exp(lam_real * step_size)
    turned = frequency * step_size
    bar_real = magnitude * jnp.cos(turned)
    bar_imag = magnitude * jnp.sin(turned)
    denom = lam_real * lam_real + frequency * frequency
    minus_one = bar_real - 1.0
    factor_real = (minus_one * lam_real + bar_imag * frequency) / denom
    factor_imag = (bar_imag * lam_real - minus_one * frequency) / denom
    b_real = factor_real[..., None] * input_real - factor_imag[..., None] * input_imag
    b_imag = factor_real[..., None] * input_imag + factor_imag[..., None] * input_real
    return (bar_real, bar_imag, b_real, b_imag)


def state_update(
    projected,
    state_real,
    state_imag,
    decay_rate,
    frequency,
    log_step,
    input_real,
    input_imag,
    output_real,
    output_imag,
    skip_gain,
):
    bar_real, bar_imag, b_real, b_imag = discretize(
        decay_rate, frequency, log_step, input_real, input_imag
    )
    count, groups, _ = state_real.shape
    high = lax.Precision.HIGHEST
    grouped = projected.astype(jnp.float32).reshape(count, groups, -1)
    drive_real = jnp.einsum("sgp,gnp->sgn", grouped, b_real, precision=high)
    drive_imag = jnp.einsum("sgp,gnp->sgn", grouped, b_imag, precision=high)
    new_real = bar_real * state_real - bar_imag * state_imag + drive_real
    new_imag = bar_real * state_imag + bar_imag * state_real + drive_imag
    readout = jnp.einsum("sgn,gpn->sgp", new_real, output_real, precision=high) - jnp.einsum(
        "sgn,gpn->sgp", new_imag, output_imag, precision=high
    )
    readout = readout.reshape(count, -1) + skip_gain * grouped.reshape(count, -1)
    return (jax.nn.gelu(readout).astype(jnp.bfloat16), new_real, new_imag)


def slot_table(own_ids, own_weights, slot_count):
    expert_range = jnp.arange(EXPERTS, dtype=jnp.int32)
    onehot = (own_ids[:, :, None] == expert_range).astype(jnp.int32)
    flat = onehot.reshape(-1, EXPERTS)
    before = (jnp.cumsum(flat, axis=0) - flat).reshape(onehot.shape)
    slots = jnp.arange(slot_count, dtype=jnp.int32)
    match = (before[..., None] == slots) & (onehot[..., None] > 0)
    table = jnp.sum(jnp.where(match, own_weights[:, :, None, None], 0.0), axis=1)
    return jnp.transpose(table, (1, 2, 0))


def shards(
    tokens,
    norm_gain,
    in_weight,
    decay_rate,
    frequency,
    log_step,
    input_real,
    input_imag,
    output_real,
    output_imag,
    skip_gain,
    state_real,
    state_imag,
    out_weight,
    ffn_gain,
    expert_ids,
    route_weights,
    gate_weight,
    up_weight,
    down_weight,
):
    normed_in = rms_scale(tokens, norm_gain).astype(jnp.bfloat16)
    projected = jnp.dot(normed_in, in_weight, preferred_element_type=jnp.float32).astype(
        jnp.bfloat16
    )
    activated, new_real, new_imag = state_update(
        projected,
        state_real,
        state_imag,
        decay_rate,
        frequency,
        log_step,
        input_real,
        input_imag,
        output_real,
        output_imag,
        skip_gain,
    )
    delta = lax.psum(jnp.dot(activated, out_weight, preferred_element_type=jnp.float32), "tp")
    hidden_state = (tokens.astype(jnp.float32) + delta).astype(jnp.bfloat16)
    normed = rms_scale(hidden_state, ffn_gain).astype(jnp.bfloat16)
    seq_count, width = normed.shape
    slot_count = seq_count // 2
    group_span = lax.axis_size("ep") // EXPERTS
    my_index = lax.axis_index("ep")
    own_ids = lax.dynamic_slice_in_dim(expert_ids, my_index * seq_count, seq_count, 0)
    unit_weights = jnp.ones(own_ids.shape, jnp.float32)
    select = slot_table(own_ids, unit_weights, slot_count)
    outgoing = jnp.einsum(
        "xcs,sd->xcd", select.astype(jnp.bfloat16), normed, preferred_element_type=jnp.float32
    ).astype(jnp.bfloat16)
    received = lax.all_to_all(
        jnp.repeat(outgoing, group_span, axis=0), "ep", split_axis=0, concat_axis=0, tiled=True
    )
    slot_rows = received.reshape(-1, width)
    gate_pre = jnp.dot(slot_rows, gate_weight, preferred_element_type=jnp.float32)
    up_pre = jnp.dot(slot_rows, up_weight, preferred_element_type=jnp.float32)
    hidden = (jax.nn.silu(gate_pre) * up_pre).astype(jnp.bfloat16)
    quarter = down_weight.shape[1]
    partial_out = jnp.dot(
        lax.all_gather(hidden, "tp", axis=1, tiled=True),
        down_weight,
        preferred_element_type=jnp.float32,
    )
    rounded = partial_out.astype(jnp.bfloat16).reshape(-1, slot_count, quarter)
    returned = lax.all_to_all(rounded, "ep", split_axis=0, concat_axis=0, tiled=True)
    summed = (
        returned.astype(jnp.float32).reshape(EXPERTS, group_span, slot_count, quarter).sum(axis=1)
    )
    weight_table = slot_table(own_ids, route_weights, slot_count)
    routed = jnp.einsum("xcs,xcd->sd", weight_table, summed, precision=lax.Precision.HIGHEST)
    residual = lax.dynamic_slice_in_dim(hidden_state, lax.axis_index("tp") * quarter, quarter, 1)
    mixed = (residual.astype(jnp.float32) + routed).astype(jnp.bfloat16)
    return (mixed, new_real, new_imag)


def solution(mesh):
    in_specs = (
        P("ep", None),
        P(),
        P(None, "tp"),
        P("tp", None),
        P("tp", None),
        P("tp"),
        P("tp", None, None),
        P("tp", None, None),
        P("tp", None, None),
        P("tp", None, None),
        P("tp"),
        P("ep", "tp", None),
        P("ep", "tp", None),
        P("tp", None),
        P(),
        P(),
        P("ep", None),
        P(None, ("ep", "tp")),
        P(None, ("ep", "tp")),
        P("ep", "tp"),
    )
    out_specs = (P("ep", "tp"), P("ep", "tp", None), P("ep", "tp", None))
    return jax.shard_map(shards, mesh=mesh, in_specs=in_specs, out_specs=out_specs, check_vma=False)
```

profile of v0, /device:TPU:0, one launch (start us, length us, event | category | flops | bytes accessed | tf_op | source)
XLA Modules:
  0.0 71.3 jit_solution(13652618909060821899)
XLA Ops:
  0.6 0.0 copy-start
  0.7 0.8 %constant_dynamic-slice_fusion = s32[4,2]{0,1:T(2,128)S(1)} fusion(s32[32,2]{0,1:T(2,128)} %param.35, s32[]{:T(128)S(6)} %select_n.14), kind=kLoop, calls=%fused_computation.78 | loop fusion | bytes 68 | tf_op jit(solution)/shard_map/dynamic_slice | solution.py:124
  1.5 0.1 copy.71
  1.6 0.1 eq.56
  1.7 0.1 fusion.42
  1.7 0.7 exp.10
  2.4 0.9 %fusion.19 = f32[4]{0:T(128)S(1)} fusion(bf16[4,2048]{1,0:T(4,128)(2,1)} %param.20), kind=kLoop, calls=%fused_computation.32 | loop fusion | flops 24572 | bytes 16400 | tf_op jit(solution)/shard_map/reduce_sum | solution.py:16
  3.3 0.7 convert_element_type.68
  4.0 1.5 %convolution_convert_fusion.2 = bf16[4,256]{1,0:T(4,128)(2,1)S(1)} fusion(bf16[2048,256]{1,0:T(8,128)(2,1)} %param.22, bf16[4,2048]{1,0:T(4,128)(2,1)} %param.20, f32[2048]{0:T(1024)S(1)} %convert_element_type.68, f32[4]{0:T(128)S(1)} %add_rsqrt_fusion.1), kind=kOutput, calls=%fused_computation.13 | convolution fusion | flops 4228096 | bytes 1075216 | tf_op jit(solution)/shard_map/dot_general | solution.py:101
  5.5 0.1 reshape.72
  5.6 0.8 %cosine_multiply_fusion = (f32[16,64]{1,0:T(8,128)S(1)}, f32[16,64]{1,0:T(8,128)S(1)}, f32[16,64]{1,0:T(8,128)S(1)}, f32[16,64]{1,0:T(8,128)S(1)}) fusion(f32[16,64]{1,0:T(8,128)} %param.24, f32[16,64]{1,0:T(8,128)} %param.23, f32[16]{0:T(128)S(1)} %exp.10), kind=kLoop, calls=%fused_computation.51 | loop fusion | flops 17408 | bytes 24640 | tf_op jit(solution)/shard_map/mul | solution.py:26
  6.4 1.2 %fusion.2 = f32[4,16,64]{2,0,1:T(4,128)S(1)} fusion(f32[16,64,16]{1,2,0:T(8,128)} %param.26, f32[16,64,16]{1,2,0:T(8,128)} %param.27, f32[16,64]{1,0:T(8,128)S(1)} %get-tuple-element.21, f32[16,64]{1,0:T(8,128)S(1)} %get-tuple-element.20, f32[4,16,64]{2,1,0:T(8,128)} %param.32, f32[4,16,64]{2,1,0:T(8,128)} %param.31, f32[16,64]{1,0:T(8,128)S(1)} %get-tuple-element.22, ...), kind=kOutput, calls=%fused_computation.6 | convolution fusion | flops 851968 | bytes 198656 | tf_op jit(solution)/shard_map/sgp,gnp->sgn/dot_general | solution.py:57
  7.6 1.2 %fusion.3 = f32[4,16,64]{2,0,1:T(4,128)S(1)} fusion(f32[16,64,16]{1,2,0:T(8,128)} %param.27, f32[16,64,16]{1,2,0:T(8,128)} %param.26, f32[16,64]{1,0:T(8,128)S(1)} %get-tuple-element.21, f32[16,64]{1,0:T(8,128)S(1)} %get-tuple-element.20, f32[4,16,64]{2,1,0:T(8,128)} %param.32, f32[4,16,64]{2,1,0:T(8,128)} %param.31, f32[16,64]{1,0:T(8,128)S(1)} %get-tuple-element.22, ...), kind=kOutput, calls=%fused_computation.8 | convolution fusion | flops 851968 | bytes 198656 | tf_op jit(solution)/shard_map/sgp,gnp->sgn/dot_general | solution.py:56
  8.8 0.1 fusion.45
  8.9 0.1 fusion.43
  9.0 0.7 convert_element_type.80
  9.7 1.2 %fusion.60 = f32[16,4,16]{2,1,0:T(4,128)S(1)} fusion(f32[4,16,64]{2,0,1:T(4,128)S(1)} %fusion.3, f32[16,16,64]{2,1,0:T(8,128)} %param.28), kind=kOutput, calls=%fused_computation.84 | convolution fusion | flops 786432 | bytes 86016 | tf_op jit(solution)/shard_map/sgn,gpn->sgp/dot_general | solution.py:60
  10.9 1.2 %fusion.1 = f32[4,16,16]{2,0,1:T(4,128)S(1)} fusion(f32[16,4,16]{2,1,0:T(4,128)S(1)} %fusion.60, f32[4,16,64]{2,0,1:T(4,128)S(1)} %fusion.2, f32[16,16,64]{2,1,0:T(8,128)} %param.29), kind=kOutput, calls=%fused_computation.4 | convolution fusion | flops 787456 | bytes 90112 | tf_op jit(solution)/shard_map/sgn,gpn->sgp/dot_general | solution.py:60
  12.1 0.1 reshape.73
  12.2 0.0 copy-done
  12.2 0.9 %fusion.46 = f32[4,2048]{1,0:T(4,128)S(1)} fusion(bf16[256,2048]{1,0:T(8,128)(2,1)S(1)} %copy-done, f32[4,256]{1,0:T(4,128)S(1)} %reshape.73, bf16[4,256]{1,0:T(4,128)(2,1)S(1)} %convolution_convert_fusion.2, f32[256]{0:T(256)} %param.30), kind=kOutput, calls=%fused_computation.69 | convolution fusion | flops 4206592 | bytes 1088512 | tf_op jit(solution)/shard_map/dot_general | solution.py:117
  13.2 12.9 %psum.7 = f32[4,2048]{1,0:T(4,128)S(1)} all-reduce(f32[4,2048]{1,0:T(4,128)S(1)} %fusion.46), channel_id=1, replica_groups=mesh['ep'=8,'tp'=4] {'tp'}, use_global_device_ids=true, to_apply=%region_1.0 | all-reduce | flops 8192 | bytes 65536 | tf_op jit(solution)/shard_map/psum | solution.py:117
  26.1 0.9 %fusion.16 = (f32[4]{0:T(128)S(1)}, bf16[4,2048]{1,0:T(4,128)(2,1)S(1)}) fusion(f32[4,2048]{1,0:T(4,128)S(1)} %psum.7, bf16[4,2048]{1,0:T(4,128)(2,1)} %param.20), kind=kLoop, calls=%fused_computation.29 | loop fusion | flops 49148 | bytes 65552 | tf_op jit(solution)/shard_map/reduce_sum | solution.py:16
  26.9 0.8 %select_reduce_fusion.1 = (f32[4,8,2]{1,0,2:T(4,128)S(1)}, bf16[4,8,2]{1,0,2:T(4,128)(2,1)S(1)}) fusion(f32[4,2]{0,1:T(2,128)} %param.36, s32[4,2,8]{2,0,1:T(4,128)S(1)} %copy.73, pred[4,2,8]{2,0,1:T(4,128)(4,1)S(1)} %copy.74), kind=kLoop, calls=%fused_computation.45 | loop fusion | flops 640 | bytes 736 | tf_op jit(solution)/shard_map/reduce_sum | solution.py:74
  27.7 0.2 convolution_convert_fusion
  27.9 0.1 copy.75
  28.0 12.5 %all_to_all.10 = bf16[8,2,2048]{2,1,0:T(2,128)(2,1)S(1)} all-to-all(bf16[8,2,2048]{2,1,0:T(2,128)(2,1)S(1)} %copy.75), channel_id=1, replica_groups=mesh['ep'=8,'tp'=4] {'ep'}, dimensions={0} | all-to-all | bytes 131072 | tf_op jit(solution)/shard_map/all_to_all | solution.py:130
  40.5 4.6 %fusion.61 = f32[16,2048]{1,0:T(8,128)S(1)} fusion(bf16[16,2048]{1,0:T(8,128)(2,1)S(1)} %reshape.74, bf16[2048,2048]{1,0:T(8,128)(2,1)} %param.37), kind=kOutput, calls=%fused_computation.85 | convolution fusion | flops 134217728 | bytes 8585216 | tf_op jit(solution)/shard_map/dot_general | solution.py:134
  45.1 4.6 %fusion = bf16[16,2048]{1,0:T(8,128)(2,1)S(1)} fusion(bf16[16,2048]{1,0:T(8,128)(2,1)S(1)} %reshape.74, bf16[2048,2048]{1,0:T(8,128)(2,1)} %param.38, f32[16,2048]{1,0:T(8,128)S(1)} %fusion.61), kind=kOutput, calls=%fused_computation.2 | convolution fusion | flops 134414336 | bytes 8650752 | tf_op jit(solution)/shard_map/dot_general | solution.py:135
  49.7 5.8 %all_gather.3 = bf16[16,8192]{1,0:T(8,128)(2,1)S(1)} all-gather(bf16[16,2048]{1,0:T(8,128)(2,1)S(1)} %fusion), channel_id=1, replica_groups=mesh['ep'=8,'tp'=4] {'tp'}, dimensions={1}, use_global_device_ids=true | all-gather | bytes 327680 | tf_op jit(solution)/shard_map/all_gather | solution.py:139
  55.5 4.6 %convolution_convert_fusion.1 = bf16[16,512]{1,0:T(8,128)(2,1)S(1)} fusion(bf16[16,8192]{1,0:T(8,128)(2,1)S(1)} %all_gather.3, bf16[8192,512]{1,0:T(8,128)(2,1)} %param.39), kind=kOutput, calls=%fused_computation.9 | convolution fusion | flops 134225920 | bytes 8667136 | tf_op jit(solution)/shard_map/dot_general | solution.py:138
  60.0 0.6 reshape.75
  60.7 3.3 %all-to-all-start.1 = ((bf16[8,2,512]{2,1,0:T(2,128)(2,1)}), bf16[8,2,512]{2,1,0:T(2,128)(2,1)S(1)}, u32[]{:S(2)}, u32[]{:S(2)}) async-start(bf16[8,2,512]{2,1,0:T(2,128)(2,1)} %reshape.75), calls=%async_computation.1 | async-start | bytes 32768 | tf_op jit(solution)/shard_map/all_to_all | solution.py:144
  64.0 0.6 copy.77
  64.6 0.6 copy.78
  65.2 5.3 %all-to-all-done.1 = bf16[8,2,512]{2,1,0:T(2,128)(2,1)S(1)} async-done(((bf16[8,2,512]{2,1,0:T(2,128)(2,1)}), bf16[8,2,512]{2,1,0:T(2,128)(2,1)S(1)}, u32[]{:S(2)}, u32[]{:S(2)}) %all-to-all-start.1) | async-done | bytes 16416 | tf_op jit(solution)/shard_map/all_to_all | solution.py:144
  70.5 0.8 %fusion.5 = bf16[4,512]{1,0:T(4,128)(2,1)} fusion(bf16[8,2,512]{2,1,0:T(2,128)(2,1)S(1)} %all-to-all-done.1, f32[4,8,2]{1,0,2:T(4,128)S(1)} %get-tuple-element.15, bf16[4,2048]{1,0:T(4,128)(2,1)S(1)} %get-tuple-element.18, s32[]{:T(128)S(6)} %select_n.13), kind=kOutput, calls=%fused_computation.12 | convolution fusion | flops 399360 | bytes 24836 | tf_op jit(solution)/shard_map/xcs,xcd->sd/dot_general | solution.py:149
  (7 shorter events, 0.1 us)
Async XLA Ops:
  0.6 11.6 %copy-start = (bf16[256,2048]{1,0:T(8,128)(2,1)S(1)}, bf16[256,2048]{1,0:T(8,128)(2,1)}, u32[]{:S(2)}) copy-start(bf16[256,2048]{1,0:T(8,128)(2,1)} %param.33) | copy-start | bytes 3145732
  60.7 9.9 %all-to-all-start.1 = ((bf16[8,2,512]{2,1,0:T(2,128)(2,1)}), bf16[8,2,512]{2,1,0:T(2,128)(2,1)S(1)}, u32[]{:S(2)}, u32[]{:S(2)}) async-start(bf16[8,2,512]{2,1,0:T(2,128)(2,1)} %reshape.75), calls=%async_computation.1 | async-start | bytes 32768 | tf_op jit(solution)/shard_map/all_to_all | solution.py:144
where the time goes:
time: 72.1 us; the launch traced here: 71.3 us
  blocking collectives  31.2 us (43%)
  matrix products  22 us (31%)
  waiting for transfers between devices  5.28 us (7%)
  other arithmetic  4.97 us (7%)
  local copies, waits for them, and re-layouts  3.84 us (5%)
  starting transfers between devices  3.33 us (5%)
  between operations  0.73 us (1%)
    psum x1, blocking collectives, shards(): lax.psum(jnp.dot(activated, out_weight, preferred_element_type=jnp.float3...  12.9 us
    all_to_all x1, blocking collectives, shards(): lax.all_to_all(jnp.repeat(outgoing, group_span, axis=0), 'ep', split_axis...  12.5 us
    all_gather x1, blocking collectives, shards(): lax.all_gather(hidden, 'tp', axis=1, tiled=True)  5.77 us
    all_to_all x1, waiting for transfers between devices, shards(): lax.all_to_all(rounded, 'ep', split_axis=0, concat_axis=0, tiled=True)  5.28 us
    dot_general x1, matrix products, shards(): up_pre = jnp.dot(slot_rows, up_weight, preferred_element_type=jnp.float32)  4.58 us
    dot_general x1, matrix products, shards(): jnp.dot(slot_rows, gate_weight, preferred_element_type=jnp.float32)  4.58 us
    dot_general x1, matrix products, shards(): jnp.dot(lax.all_gather(hidden, 'tp', axis=1, tiled=True), down_weight, pr...  4.56 us
    all_to_all x1, starting transfers between devices, shards(): lax.all_to_all(rounded, 'ep', split_axis=0, concat_axis=0, tiled=True)  3.33 us
  transfers between devices with their start and end apart: 1, of which 1 were waited for; matrix products, arithmetic and copies ran while one was open for 2% of the time, Pallas kernels for 0%

commit v1 on v0

v1 whole, which is shorter than its diff:
```python
import functools

import jax
import jax.numpy as jnp
from jax import lax
from jax.experimental import pallas as pl
from jax.experimental.pallas import tpu as pltpu
from jax.sharding import PartitionSpec as P

EXPERTS = 8
EPSILON = 1e-06
MESH = pl.DeviceIdType.MESH
F32, BF16 = jnp.float32, jnp.bfloat16
NT = (((1,), (1,)), ((), ()))


def rms_scale(floats, gain):
    return (
        floats
        * lax.rsqrt(jnp.mean(floats * floats, axis=-1, keepdims=True) + EPSILON)
        * gain.astype(F32)
    )


def mm(a, b):
    return jnp.dot(a, b, preferred_element_type=F32)


def iota(shape, axis):
    return lax.broadcasted_iota(jnp.int32, shape, axis)


def route_masks(ids, base, seqs, slots, owners, span, rows_first):
    shape = (owners * slots, 1) if rows_first else (1, owners * slots)
    place = iota(shape, 0 if rows_first else 1)
    expert, slot = place // (slots * span), place % slots
    count = jnp.zeros(shape, jnp.int32)
    masks = []
    for s in range(seqs):
        picks = []
        hit = jnp.zeros(shape, jnp.int32)
        for k in range(ids.shape[1]):
            same = jnp.where(expert == ids[base + s, k], 1, 0)
            picks.append(jnp.where(count == slot, same, 0))
            hit = hit + same
        masks.append(picks)
        count = count + hit
    return masks


def kernel(
    n_ep,
    n_tp,
    tokens_h,
    norm_gain_h,
    in_w_h,
    decay_h,
    freq_h,
    log_step_h,
    in_re_h,
    in_im_h,
    out_re_h,
    out_im_h,
    skip_h,
    st_re_h,
    st_im_h,
    out_w_h,
    ffn_gain_h,
    ids,
    weights,
    gate_h,
    up_h,
    down_h,
    mixed_o,
    new_re_o,
    new_im_o,
    tokens_v,
    norm_gain_v,
    in_w_v,
    decay_v,
    freq_v,
    log_step_v,
    in_re_v,
    in_im_v,
    out_re_v,
    out_im_v,
    skip_v,
    st_re_v,
    st_im_v,
    out_w_v,
    ffn_gain_v,
    gate_v,
    up_v,
    down_v,
    bt_v,
    part_v,
    hidden_v,
    xs_v,
    x_v,
    outg_v,
    recvd_v,
    hid_v,
    ys_v,
    retg_v,
    retd_v,
    load_sem,
    gate_sem,
    up_sem,
    down_sem,
    part_send,
    part_recv,
    disp_send,
    disp_recv,
    hid_send,
    hid_recv,
    ret_send,
    ret_recv,
):
    ep, tp = lax.axis_index("ep"), lax.axis_index("tp")
    chunks, _, cw = gate_v.shape
    seqs, width = tokens_v.shape
    groups, states = decay_v.shape
    chan = in_re_v.shape[2]
    slots = seqs // 2
    span = n_ep // EXPERTS
    rows = n_ep * slots
    quarter = down_v.shape[1]
    piece = chunks * cw

    def tp_peer(d):
        return (tp // 2 * 2 + d // 2 * 2) % n_tp + (tp % 2 + d % 2) % 2

    def ep_to(d):
        return (ep + d) % n_ep

    def ep_from(d):
        return (ep + n_ep - d) % n_ep

    pairs = [
        (tokens_h, tokens_v),
        (norm_gain_h, norm_gain_v),
        (in_w_h, in_w_v),
        (in_re_h, in_re_v),
        (in_im_h, in_im_v),
        (log_step_h, log_step_v),
        (decay_h, decay_v),
        (freq_h, freq_v),
        (st_re_h, st_re_v),
        (st_im_h, st_im_v),
        (out_re_h, out_re_v),
        (out_im_h, out_im_v),
        (skip_h, skip_v),
        (out_w_h, out_w_v),
        (ffn_gain_h, ffn_gain_v),
    ]
    loads = [pltpu.make_async_copy(a, b, load_sem.at[i]) for i, (a, b) in enumerate(pairs)]
    for load in loads:
        load.start()

    barrier = pltpu.get_barrier_semaphore()
    for d in range(1, n_tp):
        pl.semaphore_signal(barrier, inc=1, device_id={"tp": tp_peer(d)}, device_id_type=MESH)
    for d in range(1, n_ep):
        pl.semaphore_signal(barrier, inc=1, device_id={"ep": ep_to(d)}, device_id_type=MESH)

    def gate_copy(c):
        cols = pl.ds(pl.multiple_of(c * cw, cw), cw)
        return (
            pltpu.make_async_copy(gate_h.at[:, cols], gate_v.at[c], gate_sem.at[c]),
            pltpu.make_async_copy(up_h.at[:, cols], up_v.at[c], up_sem.at[c]),
        )

    def down_copy(p):
        part = pl.ds(pl.multiple_of(p * piece, piece), piece)
        return pltpu.make_async_copy(down_h.at[part], down_v.at[part], down_sem.at[p])

    for c in range(chunks):
        for copy in gate_copy(c):
            copy.start()
    for d in range(n_tp):
        down_copy(tp_peer(d)).start()

    for load in loads[3:8]:
        load.wait()
    ident = (iota((chan, chan), 0) == iota((chan, chan), 1)).astype(BF16)

    def turn(g, _):
        both = jnp.concatenate([in_re_v[g], in_im_v[g]], axis=0).astype(BF16)
        bt_v[g] = lax.dot_general(ident, both, NT, preferred_element_type=F32).astype(BF16)
        return 0

    lax.fori_loop(0, groups, turn, 0)
    eye = iota((groups, groups), 0) == iota((groups, groups), 1)
    step_size = jnp.sum(jnp.where(eye, jnp.exp(log_step_v[...]), 0.0), axis=1, keepdims=True)
    lam_real, frequency = -decay_v[...], freq_v[...]
    magnitude = jnp.exp(lam_real * step_size)
    turned = frequency * step_size
    bar_real = magnitude * jnp.cos(turned)
    bar_imag = magnitude * jnp.sin(turned)
    denom = lam_real * lam_real + frequency * frequency
    minus_one = bar_real - 1.0
    factor_real = (minus_one * lam_real + bar_imag * frequency) / denom
    factor_imag = (bar_imag * lam_real - minus_one * frequency) / denom

    def per_seq(values):
        return jnp.concatenate([values] * seqs, axis=0)

    for load in loads[0:3]:
        load.wait()
    floats = tokens_v[...].astype(F32)
    normed_in = rms_scale(floats, norm_gain_v[...]).astype(BF16)
    projected = mm(normed_in, in_w_v[...]).astype(BF16).astype(F32)
    channels = projected.shape[1]
    own = iota((groups, channels), 1) // chan == iota((groups, channels), 0)
    spread = jnp.concatenate(
        [
            jnp.where(own, jnp.broadcast_to(projected[s : s + 1], own.shape), 0.0)
            for s in range(seqs)
        ],
        axis=0,
    ).astype(BF16)
    drive = mm(spread, bt_v[...].reshape(channels, 2 * states))
    drive_real, drive_imag = drive[:, :states], drive[:, states:]
    for load in loads[8:13]:
        load.wait()
    sr = st_re_v[...].reshape(seqs * groups, states)
    si = st_im_v[...].reshape(seqs * groups, states)
    br, bi, fr, fi = map(per_seq, (bar_real, bar_imag, factor_real, factor_imag))
    new_real = br * sr - bi * si + (fr * drive_real - fi * drive_imag)
    new_imag = br * si + bi * sr + (fr * drive_imag + fi * drive_real)
    new_re_o[...] = new_real.reshape(seqs, groups, states)
    new_im_o[...] = new_imag.reshape(seqs, groups, states)
    out_re = out_re_v[...].reshape(channels, states).astype(BF16)
    out_im = out_im_v[...].reshape(channels, states).astype(BF16)
    full = lax.dot_general(
        new_real.astype(BF16), out_re, NT, preferred_element_type=F32
    ) - lax.dot_general(new_imag.astype(BF16), out_im, NT, preferred_element_type=F32)
    readout = jnp.concatenate(
        [
            jnp.sum(
                jnp.where(own, full[s * groups : (s + 1) * groups], 0.0), axis=0, keepdims=True
            )
            for s in range(seqs)
        ],
        axis=0,
    )
    readout = readout + skip_v[...] * projected
    activated = jax.nn.gelu(readout).astype(BF16)
    loads[13].wait()
    part_v[tp] = mm(activated, out_w_v[...]).astype(BF16)

    def part_copy(d):
        return pltpu.make_async_remote_copy(
            src_ref=part_v.at[tp],
            dst_ref=part_v.at[tp],
            send_sem=part_send.at[d],
            recv_sem=part_recv.at[tp],
            device_id={"tp": tp_peer(d)},
            device_id_type=MESH,
        )

    def part_arrival(d):
        p = tp_peer(d)
        return pltpu.make_async_remote_copy(
            src_ref=part_v.at[p],
            dst_ref=part_v.at[p],
            send_sem=part_send.at[d],
            recv_sem=part_recv.at[p],
            device_id={"tp": p},
            device_id_type=MESH,
        )

    pl.semaphore_wait(barrier, n_tp - 1 + n_ep - 1)
    for d in range(n_tp - 1, 0, -1):
        part_copy(d).start()

    base = ep * seqs
    by_row = route_masks(ids, base, seqs, slots, n_ep, span, True)
    by_lane = route_masks(ids, base, seqs, slots, n_ep, span, False)
    seq_lane, seq_row = iota((rows, seqs), 1), iota((seqs, rows), 0)
    select = jnp.zeros((rows, seqs), F32)
    table = jnp.zeros((seqs, rows), F32)
    for s in range(seqs):
        picked = functools.reduce(lambda a, b: a + b, by_row[s]).astype(F32)
        select = jnp.where(seq_lane == s, picked, select)
        weighed = functools.reduce(
            lambda a, b: a + b,
            [pick.astype(F32) * weights[s, k] for k, pick in enumerate(by_lane[s])],
        )
        table = jnp.where(seq_row == s, weighed, table)
    select = select.astype(BF16)

    loads[14].wait()
    for d in range(1, n_tp):
        part_arrival(d).wait_recv()
    delta = jnp.zeros((seqs, width), F32)
    for t in range(n_tp):
        delta = delta + part_v[t].astype(F32)
    hidden_state = (floats + delta).astype(BF16).astype(F32)
    hidden_v[...] = hidden_state
    normed = rms_scale(hidden_state, ffn_gain_v[...]).astype(BF16)
    xs_v[...] = mm(select, normed)
    for j in range(n_ep):
        outg_v[j] = xs_v[j * slots : (j + 1) * slots, :].astype(BF16)

    def swap(source, target, send, recv, d):
        return pltpu.make_async_remote_copy(
            src_ref=source.at[ep_to(d)],
            dst_ref=target.at[ep],
            send_sem=send.at[d],
            recv_sem=recv.at[ep],
            device_id={"ep": ep_to(d)},
            device_id_type=MESH,
        )

    def arrival(source, target, send, recv, d):
        j = ep_from(d)
        return pltpu.make_async_remote_copy(
            src_ref=source.at[j],
            dst_ref=target.at[j],
            send_sem=send.at[d],
            recv_sem=recv.at[j],
            device_id={"ep": j},
            device_id_type=MESH,
        )

    there = (outg_v, recvd_v, disp_send, disp_recv)
    back = (retg_v, retd_v, ret_send, ret_recv)
    for d in range(1, n_ep):
        swap(*there, d).start()
    recvd_v[ep] = outg_v[ep]
    for d in range(1, n_ep):
        arrival(*there, d).wait_recv()
    for j in range(n_ep):
        xs_v[j * slots : (j + 1) * slots, :] = recvd_v[j].astype(F32)
    x_v[...] = xs_v[...].astype(BF16)

    def hid_copy(c, d):
        return pltpu.make_async_remote_copy(
            src_ref=hid_v.at[tp, c],
            dst_ref=hid_v.at[tp, c],
            send_sem=hid_send.at[d, c],
            recv_sem=hid_recv.at[tp, c],
            device_id={"tp": tp_peer(d)},
            device_id_type=MESH,
        )

    def hid_arrival(c, d):
        p = tp_peer(d)
        return pltpu.make_async_remote_copy(
            src_ref=hid_v.at[p, c],
            dst_ref=hid_v.at[p, c],
            send_sem=hid_send.at[d, c],
            recv_sem=hid_recv.at[p, c],
            device_id={"tp": p},
            device_id_type=MESH,
        )

    def expand(c, _):
        for copy in gate_copy(c):
            copy.wait()
        x = x_v[...]
        gate_pre = mm(x, gate_v[c])
        up_pre = mm(x, up_v[c])
        hid_v[tp, c] = (jax.nn.silu(gate_pre) * up_pre).astype(BF16)
        for d in range(n_tp - 1, 0, -1):
            hid_copy(c, d).start()
        return 0

    lax.fori_loop(0, chunks, expand, 0)

    def contract(c, d):
        p = tp_peer(d)
        start = pl.multiple_of(p * piece + c * cw, cw)
        return mm(hid_v[p, c], down_v[pl.ds(start, cw), :])

    ys_v[...] = jnp.zeros_like(ys_v)
    for group in ([0], [1], list(range(2, n_tp))):
        for d in group:
            down_copy(tp_peer(d)).wait()

        def shrink(c, _, group=group):
            for d in group:
                if d > 0:
                    hid_arrival(c, d).wait_recv()
                ys_v[...] += contract(c, d)
            return 0

        lax.fori_loop(0, chunks, shrink, 0)

    for j in range(n_ep):
        retg_v[j] = ys_v[j * slots : (j + 1) * slots, :].astype(BF16)
    for d in range(1, n_ep):
        swap(*back, d).start()
    retd_v[ep] = retg_v[ep]
    for d in range(1, n_tp):
        part_copy(d).wait_send()
    for d in range(1, n_ep):
        swap(*there, d).wait_send()

    def sent(c, _):
        for d in range(1, n_tp):
            hid_copy(c, d).wait_send()
        return 0

    lax.fori_loop(0, chunks, sent, 0)
    residual = hidden_v[:, pl.ds(pl.multiple_of(tp * quarter, quarter), quarter)]
    for d in range(1, n_ep):
        arrival(*back, d).wait_recv()
    for j in range(n_ep):
        ys_v[j * slots : (j + 1) * slots, :] = retd_v[j].astype(F32)
    routed = jnp.dot(
        table, ys_v[...], preferred_element_type=F32, precision=lax.Precision.HIGHEST
    )
    mixed_o[...] = (residual + routed).astype(BF16)
    for d in range(1, n_ep):
        swap(*back, d).wait_send()


def shards(
    tokens,
    norm_gain,
    in_weight,
    decay_rate,
    frequency,
    log_step,
    input_real,
    input_imag,
    output_real,
    output_imag,
    skip_gain,
    state_real,
    state_imag,
    out_weight,
    ffn_gain,
    expert_ids,
    route_weights,
    gate_weight,
    up_weight,
    down_weight,
):
    n_ep, n_tp = lax.axis_size("ep"), lax.axis_size("tp")
    seqs, width = tokens.shape
    slots = seqs // 2
    rows = n_ep * slots
    columns = gate_weight.shape[1]
    cw = min(512, columns)
    chunks = columns // cw
    quarter = down_weight.shape[1]
    groups, states, chan = input_real.shape
    operands = [
        tokens,
        norm_gain.reshape(1, -1),
        in_weight,
        decay_rate,
        frequency,
        log_step.reshape(1, -1),
        input_real,
        input_imag,
        output_real,
        output_imag,
        skip_gain.reshape(1, -1),
        state_real,
        state_imag,
        out_weight,
        ffn_gain.reshape(1, -1),
        expert_ids,
        route_weights,
        gate_weight,
        up_weight,
        down_weight,
    ]
    any_spec = pl.BlockSpec(memory_space=pl.ANY)
    smem = pl.BlockSpec(memory_space=pltpu.SMEM)
    vmem = pl.BlockSpec(memory_space=pltpu.VMEM)
    dma = pltpu.SemaphoreType.DMA
    copies = [pltpu.VMEM(value.shape, value.dtype) for value in operands[:15]]
    return pl.pallas_call(
        functools.partial(kernel, n_ep, n_tp),
        out_shape=(
            jax.ShapeDtypeStruct((seqs, quarter), BF16),
            jax.ShapeDtypeStruct(state_real.shape, F32),
            jax.ShapeDtypeStruct(state_imag.shape, F32),
        ),
        in_specs=[any_spec] * 15 + [smem] * 2 + [any_spec] * 3,
        out_specs=(vmem, vmem, vmem),
        scratch_shapes=copies
        + [
            pltpu.VMEM((chunks, width, cw), BF16),
            pltpu.VMEM((chunks, width, cw), BF16),
            pltpu.VMEM(down_weight.shape, BF16),
            pltpu.VMEM((groups, chan, 2 * states), BF16),
            pltpu.VMEM((n_tp, seqs, width), BF16),
            pltpu.VMEM((seqs, width), F32),
            pltpu.VMEM((rows, width), F32),
            pltpu.VMEM((rows, width), BF16),
            pltpu.VMEM((n_ep, slots, width), BF16),
            pltpu.VMEM((n_ep, slots, width), BF16),
            pltpu.VMEM((n_tp, chunks, rows, cw), BF16),
            pltpu.VMEM((rows, quarter), F32),
            pltpu.VMEM((n_ep, slots, quarter), BF16),
            pltpu.VMEM((n_ep, slots, quarter), BF16),
            dma((15,)),
            dma((chunks,)),
            dma((chunks,)),
            dma((n_tp,)),
            dma((n_tp,)),
            dma((n_tp,)),
            dma((n_ep,)),
            dma((n_ep,)),
            dma((n_tp, chunks)),
            dma((n_tp, chunks)),
            dma((n_ep,)),
            dma((n_ep,)),
        ],
        compiler_params=pltpu.CompilerParams(
            collective_id=0, has_side_effects=True, vmem_limit_bytes=60 * 1024 * 1024
        ),
        name="layer",
    )(*operands)


def solution(mesh):
    in_specs = (
        P("ep", None),
        P(),
        P(None, "tp"),
        P("tp", None),
        P("tp", None),
        P("tp"),
        P("tp", None, None),
        P("tp", None, None),
        P("tp", None, None),
        P("tp", None, None),
        P("tp"),
        P("ep", "tp", None),
        P("ep", "tp", None),
        P("tp", None),
        P(),
        P(),
        P("ep", None),
        P(None, ("ep", "tp")),
        P(None, ("ep", "tp")),
        P("ep", "tp"),
    )
    out_specs = (P("ep", "tp"), P("ep", "tp", None), P("ep", "tp", None))
    return jax.shard_map(shards, mesh=mesh, in_specs=in_specs, out_specs=out_specs, check_vma=False)
```

time: 72.1 us -> 41.5 us (0.58)
  blocking collectives: 31.2 us -> 0 us
  Pallas kernels: 0 us -> 27.2 us
  matrix products: 22 us -> 0 us
  local copies, waits for them, and re-layouts: 3.84 us -> 13.1 us
  waiting for transfers between devices: 5.28 us -> 0 us
  other arithmetic: 4.97 us -> 0 us
  starting transfers between devices: 3.33 us -> 0 us
    pallas_call x0 -> x1, Pallas kernels: none -> 27.2 us  [shards(): pl.pallas_call(functools.partial(kernel, n_ep, n_tp), out_shape=(jax.Shap...]
    dot_general x11 -> x0, matrix products: 22 us -> none  [the longest x1 4.58 us: shards(): up_pre = jnp.dot(slot_rows, up_weight, preferred_element_type=jnp.float32)]
    psum x1 -> x0, blocking collectives: 12.9 us -> none  [shards(): lax.psum(jnp.dot(activated, out_weight, preferred_element_type=jnp.float3...]
    all_to_all x1 -> x0, blocking collectives: 12.5 us -> none  [shards(): lax.all_to_all(jnp.repeat(outgoing, group_span, axis=0), 'ep', split_axis...]
    unnamed x4 -> x7, local copies, waits for them, and re-layouts: 1.24 us -> 10.5 us
    all_gather x1 -> x0, blocking collectives: 5.77 us -> none  [shards(): lax.all_gather(hidden, 'tp', axis=1, tiled=True)]
    all_to_all x1 -> x0, waiting for transfers between devices: 5.28 us -> none  [shards(): lax.all_to_all(rounded, 'ep', split_axis=0, concat_axis=0, tiled=True)]
    all_to_all x1 -> x0, starting transfers between devices: 3.33 us -> none  [shards(): lax.all_to_all(rounded, 'ep', split_axis=0, concat_axis=0, tiled=True)]
  transfers between devices with their start and end apart: 1 -> 0, of which waited for: 1 -> 0; matrix products, arithmetic and copies ran while one was open for 2% -> 0% of each run, Pallas kernels for 0% -> 0%
where the time goes in v1:
time: 41.5 us; the launch traced here: 41 us
  Pallas kernels  27.2 us (66%)
  local copies, waits for them, and re-layouts  13.1 us (32%)
  between operations  0.64 us (2%)
    pallas_call x1, Pallas kernels, shards(): pl.pallas_call(functools.partial(kernel, n_ep, n_tp), out_shape=(jax.Shap...  27.2 us
    unnamed x7, local copies, waits for them, and re-layouts  10.5 us
    reshape x1, local copies, waits for them, and re-layouts, shards(): norm_gain.reshape(1, -1)  1.29 us
    reshape x1, local copies, waits for them, and re-layouts, shards(): ffn_gain.reshape(1, -1)  1.29 us

profile of v1, /device:TPU:0, one launch (start us, length us, event | category | flops | bytes accessed | tf_op | source)
XLA Modules:
  0.0 41.0 jit_solution(10697776279203027049)
XLA Ops:
  0.6 1.3 %copy.26.weights = f32[4,2]{1,0:T(4,128)} copy(f32[4,2]{0,1:T(2,128)} %param.36) | data formatting | bytes 64 | tf_op args[16]
  2.0 1.3 %reshape.18.norm_gain_h = bf16[1,2048]{1,0:T(2,128)(2,1)} reshape(bf16[2048]{0:T(1024)(128)(2,1)} %param.21) | data formatting | bytes 8192 | tf_op jit(solution)/shard_map/reshape | solution.py:453
  3.3 1.3 %reshape.21.ffn_gain_h = bf16[1,2048]{1,0:T(2,128)(2,1)} reshape(bf16[2048]{0:T(1024)(128)(2,1)} %param.34) | data formatting | bytes 8192 | tf_op jit(solution)/shard_map/reshape | solution.py:466
  4.5 1.4 %copy.25.ids = s32[32,2]{1,0:T(8,128)} copy(s32[32,2]{0,1:T(2,128)} %param.35) | data formatting | bytes 512 | tf_op args[15]
  5.9 1.9 %copy.23.in_re_h = f32[16,64,16]{2,1,0:T(8,128)} copy(f32[16,64,16]{1,2,0:T(8,128)} %param.26) | data formatting | bytes 131072 | tf_op args[6]
  7.8 1.9 %copy.24.in_im_h = f32[16,64,16]{2,1,0:T(8,128)} copy(f32[16,64,16]{1,2,0:T(8,128)} %param.27) | data formatting | bytes 131072 | tf_op args[7]
  9.7 27.2 %layer.1 = (bf16[4,512]{1,0:T(4,128)(2,1)}, f32[4,16,64]{2,1,0:T(8,128)}, f32[4,16,64]{2,1,0:T(8,128)}) custom-call(bf16[4,2048]{1,0:T(4,128)(2,1)} %tokens_h.1, bf16[1,2048]{1,0:T(2,128)(2,1)} %reshape.18.norm_gain_h, bf16[2048,256]{1,0:T(8,128)(2,1)} %in_w_h.1, f32[16,64]{1,0:T(8,128)} %decay_h.1, f32[16,64]{1,0:T(8,128)} %freq_h.1, f32[1,16]{1,0:T(1,128)} %bitcast.3, ...), custom_call_target="tpu_custom_call" | custom-call | tf_op jit(solution)/shard_map/layer/pallas_call | solution.py:478
  37.0 1.3 %copy.30 = bf16[4,512]{1,0:T(4,128)(2,1)} copy(bf16[4,512]{1,0:T(4,128)(2,1)} %get-tuple-element.6) | data formatting | bytes 8192
  38.2 1.4 %copy.31 = f32[4,16,64]{2,1,0:T(8,128)} copy(f32[4,16,64]{2,1,0:T(8,128)} %get-tuple-element.7) | data formatting | bytes 32768
  39.6 1.4 %copy.32 = f32[4,16,64]{2,1,0:T(8,128)} copy(f32[4,16,64]{2,1,0:T(8,128)} %get-tuple-element.8) | data formatting | bytes 32768

commit v2 on v1

--- a/solution.py
+++ b/solution.py
@@ -18,8 +18,13 @@
     return (
         floats
         * lax.rsqrt(jnp.mean(floats * floats, axis=-1, keepdims=True) + EPSILON)
-        * gain.astype(F32)
+        * gain
     )
+
+
+def flat_row(ref):
+    values = ref[...].astype(F32)
+    return jnp.concatenate([values[i : i + 1] for i in range(values.shape[0])], axis=1)
 
 
 def mm(a, b):
@@ -39,8 +44,8 @@
     for s in range(seqs):
         picks = []
         hit = jnp.zeros(shape, jnp.int32)
-        for k in range(ids.shape[1]):
-            same = jnp.where(expert == ids[base + s, k], 1, 0)
+        for k in range(ids.shape[0]):
+            same = jnp.where(expert == ids[k, base + s], 1, 0)
             picks.append(jnp.where(count == slot, same, 0))
             hit = hit + same
         masks.append(picks)
@@ -92,7 +97,6 @@
     gate_v,
     up_v,
     down_v,
-    bt_v,
     part_v,
     hidden_v,
     xs_v,
@@ -120,7 +124,7 @@
     chunks, _, cw = gate_v.shape
     seqs, width = tokens_v.shape
     groups, states = decay_v.shape
-    chan = in_re_v.shape[2]
+    chan = in_re_v.shape[1]
     slots = seqs // 2
     span = n_ep // EXPERTS
     rows = n_ep * slots
@@ -182,14 +186,6 @@
 
     for load in loads[3:8]:
         load.wait()
-    ident = (iota((chan, chan), 0) == iota((chan, chan), 1)).astype(BF16)
-
-    def turn(g, _):
-        both = jnp.concatenate([in_re_v[g], in_im_v[g]], axis=0).astype(BF16)
-        bt_v[g] = lax.dot_general(ident, both, NT, preferred_element_type=F32).astype(BF16)
-        return 0
-
-    lax.fori_loop(0, groups, turn, 0)
     eye = iota((groups, groups), 0) == iota((groups, groups), 1)
     step_size = jnp.sum(jnp.where(eye, jnp.exp(log_step_v[...]), 0.0), axis=1, keepdims=True)
     lam_real, frequency = -decay_v[...], freq_v[...]
@@ -208,7 +204,7 @@
     for load in loads[0:3]:
         load.wait()
     floats = tokens_v[...].astype(F32)
-    normed_in = rms_scale(floats, norm_gain_v[...]).astype(BF16)
+    normed_in = rms_scale(floats, flat_row(norm_gain_v)).astype(BF16)
     projected = mm(normed_in, in_w_v[...]).astype(BF16).astype(F32)
     channels = projected.shape[1]
     own = iota((groups, channels), 1) // chan == iota((groups, channels), 0)
@@ -219,8 +215,8 @@
         ],
         axis=0,
     ).astype(BF16)
-    drive = mm(spread, bt_v[...].reshape(channels, 2 * states))
-    drive_real, drive_imag = drive[:, :states], drive[:, states:]
+    drive_real = mm(spread, in_re_v[...].reshape(channels, states).astype(BF16))
+    drive_imag = mm(spread, in_im_v[...].reshape(channels, states).astype(BF16))
     for load in loads[8:13]:
         load.wait()
     sr = st_re_v[...].reshape(seqs * groups, states)
@@ -285,12 +281,13 @@
         select = jnp.where(seq_lane == s, picked, select)
         weighed = functools.reduce(
             lambda a, b: a + b,
-            [pick.astype(F32) * weights[s, k] for k, pick in enumerate(by_lane[s])],
+            [pick.astype(F32) * weights[k, s] for k, pick in enumerate(by_lane[s])],
         )
         table = jnp.where(seq_row == s, weighed, table)
     select = select.astype(BF16)
 
     loads[14].wait()
+    ffn_gain = flat_row(ffn_gain_v)
     for d in range(1, n_tp):
         part_arrival(d).wait_recv()
     delta = jnp.zeros((seqs, width), F32)
@@ -298,7 +295,7 @@
         delta = delta + part_v[t].astype(F32)
     hidden_state = (floats + delta).astype(BF16).astype(F32)
     hidden_v[...] = hidden_state
-    normed = rms_scale(hidden_state, ffn_gain_v[...]).astype(BF16)
+    normed = rms_scale(hidden_state, ffn_gain).astype(BF16)
     xs_v[...] = mm(select, normed)
     for j in range(n_ep):
         outg_v[j] = xs_v[j * slots : (j + 1) * slots, :].astype(BF16)
@@ -415,6 +412,11 @@
     mixed_o[...] = (residual + routed).astype(BF16)
     for d in range(1, n_ep):
         swap(*back, d).wait_send()
+
+
+def hand_over(*refs):
+    for source, target in zip(refs[:3], refs[3:]):
+        target[...] = source[...]
 
 
 def shards(
@@ -447,25 +449,24 @@
     cw = min(512, columns)
     chunks = columns // cw
     quarter = down_weight.shape[1]
-    groups, states, chan = input_real.shape
     operands = [
         tokens,
-        norm_gain.reshape(1, -1),
+        norm_gain.reshape(-1, 128),
         in_weight,
         decay_rate,
         frequency,
         log_step.reshape(1, -1),
-        input_real,
-        input_imag,
+        jnp.swapaxes(input_real, 1, 2),
+        jnp.swapaxes(input_imag, 1, 2),
         output_real,
         output_imag,
         skip_gain.reshape(1, -1),
         state_real,
         state_imag,
         out_weight,
-        ffn_gain.reshape(1, -1),
-        expert_ids,
-        route_weights,
+        ffn_gain.reshape(-1, 128),
+        expert_ids.T,
+        route_weights.T,
         gate_weight,
         up_weight,
         down_weight,
@@ -475,7 +476,7 @@
     vmem = pl.BlockSpec(memory_space=pltpu.VMEM)
     dma = pltpu.SemaphoreType.DMA
     copies = [pltpu.VMEM(value.shape, value.dtype) for value in operands[:15]]
-    return pl.pallas_call(
+    results = pl.pallas_call(
         functools.partial(kernel, n_ep, n_tp),
         out_shape=(
             jax.ShapeDtypeStruct((seqs, quarter), BF16),
@@ -489,7 +490,6 @@
             pltpu.VMEM((chunks, width, cw), BF16),
             pltpu.VMEM((chunks, width, cw), BF16),
             pltpu.VMEM(down_weight.shape, BF16),
-            pltpu.VMEM((groups, chan, 2 * states), BF16),
             pltpu.VMEM((n_tp, seqs, width), BF16),
             pltpu.VMEM((seqs, width), F32),
             pltpu.VMEM((rows, width), F32),
@@ -518,6 +518,13 @@
         ),
         name="layer",
     )(*operands)
+    return pl.pallas_call(
+        hand_over,
+        out_shape=tuple(jax.ShapeDtypeStruct(r.shape, r.dtype) for r in results),
+        in_specs=[vmem] * 3,
+        out_specs=(vmem,) * 3,
+        name="hand_over",
+    )(*results)
 
 
 def solution(mesh):

time: 41.5 us -> 28.2 us (0.68)
  local copies, waits for them, and re-layouts: 13.1 us -> 0 us
    unnamed x7 -> x0, local copies, waits for them, and re-layouts: 10.5 us -> none
    reshape x2 -> x0, local copies, waits for them, and re-layouts: 2.58 us -> none  [the longest x1 1.29 us: shards(): norm_gain.reshape(1, -1)]
    pallas_call x0 -> x1, Pallas kernels: none -> 1.41 us  [shards(): pl.pallas_call(hand_over, out_shape=tuple((jax.ShapeDtypeStruct(r.shape,...]
    pallas_call x1, Pallas kernels: 27.2 us -> 25.9 us  [shards(): pl.pallas_call(functools.partial(kernel, n_ep, n_tp), out_shape=(jax.Shap...]
where the time goes in v2:
time: 28.2 us; the launch traced here: 28 us
  Pallas kernels  27.3 us (97%)
  between operations  0.65 us (2%)
    pallas_call x1, Pallas kernels, shards(): pl.pallas_call(functools.partial(kernel, n_ep, n_tp), out_shape=(jax.Shap...  25.9 us
    pallas_call x1, Pallas kernels, shards(): pl.pallas_call(hand_over, out_shape=tuple((jax.ShapeDtypeStruct(r.shape,...  1.41 us

profile of v2, /device:TPU:0, one launch (start us, length us, event | category | flops | bytes accessed | tf_op | source)
XLA Modules:
  0.0 28.0 jit_solution(2843476072335102203)
XLA Ops:
  0.6 25.9 %layer.1 = (bf16[4,512]{1,0:T(4,128)(2,1)}, f32[4,16,64]{2,1,0:T(8,128)}, f32[4,16,64]{2,1,0:T(8,128)}) custom-call(bf16[4,2048]{1,0:T(4,128)(2,1)} %tokens_h.1, bf16[16,128]{1,0:T(8,128)(2,1)} %bitcast.10, bf16[2048,256]{1,0:T(8,128)(2,1)} %in_w_h.1, f32[16,64]{1,0:T(8,128)} %decay_h.1, f32[16,64]{1,0:T(8,128)} %freq_h.1, f32[1,16]{1,0:T(1,128)} %bitcast.15, ...), custom_call_target="tpu_custom_call" | custom-call | tf_op jit(solution)/shard_map/layer/pallas_call | solution.py:479
  26.6 1.4 %hand_over.1 = (bf16[4,512]{1,0:T(4,128)(2,1)}, f32[4,16,64]{2,1,0:T(8,128)}, f32[4,16,64]{2,1,0:T(8,128)}) custom-call(bf16[4,512]{1,0:T(4,128)(2,1)} %get-tuple-element.6.refs_0_, f32[4,16,64]{2,1,0:T(8,128)} %get-tuple-element.7.refs_1_, f32[4,16,64]{2,1,0:T(8,128)} %get-tuple-element.8.refs_2_), custom_call_target="tpu_custom_call" | custom-call | tf_op jit(solution)/shard_map/hand_over/pallas_call | solution.py:521

commit v3 on v2

--- a/solution.py
+++ b/solution.py
@@ -178,12 +178,6 @@
         part = pl.ds(pl.multiple_of(p * piece, piece), piece)
         return pltpu.make_async_copy(down_h.at[part], down_v.at[part], down_sem.at[p])
 
-    for c in range(chunks):
-        for copy in gate_copy(c):
-            copy.start()
-    for d in range(n_tp):
-        down_copy(tp_peer(d)).start()
-
     for load in loads[3:8]:
         load.wait()
     eye = iota((groups, groups), 0) == iota((groups, groups), 1)
@@ -203,6 +197,11 @@
 
     for load in loads[0:3]:
         load.wait()
+    for c in range(chunks):
+        for copy in gate_copy(c):
+            copy.start()
+    for d in range(n_tp):
+        down_copy(tp_peer(d)).start()
     floats = tokens_v[...].astype(F32)
     normed_in = rms_scale(floats, flat_row(norm_gain_v)).astype(BF16)
     projected = mm(normed_in, in_w_v[...]).astype(BF16).astype(F32)

time: 28.2 us -> 28.2 us (level)
  no operation moved by 1% of the time
where the time goes in v3:
time: 28.2 us; the launch traced here: 28 us
  Pallas kernels  27.3 us (97%)
  between operations  0.65 us (2%)
    pallas_call x1, Pallas kernels, shards(): pl.pallas_call(functools.partial(kernel, n_ep, n_tp), out_shape=(jax.Shap...  25.9 us
    pallas_call x1, Pallas kernels, shards(): pl.pallas_call(hand_over, out_shape=tuple((jax.ShapeDtypeStruct(r.shape,...  1.41 us

profile of v3, /device:TPU:0, one launch (start us, length us, event | category | flops | bytes accessed | tf_op | source)
XLA Modules:
  0.0 28.0 jit_solution(6691709883070950117)
XLA Ops:
  0.6 25.9 %layer.1 = (bf16[4,512]{1,0:T(4,128)(2,1)}, f32[4,16,64]{2,1,0:T(8,128)}, f32[4,16,64]{2,1,0:T(8,128)}) custom-call(bf16[4,2048]{1,0:T(4,128)(2,1)} %tokens_h.1, bf16[16,128]{1,0:T(8,128)(2,1)} %bitcast.10, bf16[2048,256]{1,0:T(8,128)(2,1)} %in_w_h.1, f32[16,64]{1,0:T(8,128)} %decay_h.1, f32[16,64]{1,0:T(8,128)} %freq_h.1, f32[1,16]{1,0:T(1,128)} %bitcast.15, ...), custom_call_target="tpu_custom_call" | custom-call | tf_op jit(solution)/shard_map/layer/pallas_call | solution.py:478
  26.6 1.4 %hand_over.1 = (bf16[4,512]{1,0:T(4,128)(2,1)}, f32[4,16,64]{2,1,0:T(8,128)}, f32[4,16,64]{2,1,0:T(8,128)}) custom-call(bf16[4,512]{1,0:T(4,128)(2,1)} %get-tuple-element.6.refs_0_, f32[4,16,64]{2,1,0:T(8,128)} %get-tuple-element.7.refs_1_, f32[4,16,64]{2,1,0:T(8,128)} %get-tuple-element.8.refs_2_), custom_call_target="tpu_custom_call" | custom-call | tf_op jit(solution)/shard_map/hand_over/pallas_call | solution.py:520
